TPU v7x, 512 devices: a whole 4x4x16 slice. The times are simulated.
512 devices in a mesh: kv: 64 (over z, y), tp: 8 (over x, core).
Axes of the slice: x: 4, y: 4, z: 16, core: 2. Of those that a mesh axis runs over, the one named last changes fastest.
Arguments:
- tokens: bfloat16 [24576, 2048], P('kv', 'tp'), may hold values from -12 to 12
- query_weight: bfloat16 [2048, 2048], P(None, 'tp'), may hold values from -0.5 to 0.5
- key_weight: bfloat16 [2048, 1024], P(None, 'tp'), may hold values from -0.5 to 0.5
- value_weight: bfloat16 [2048, 1024], P(None, 'tp'), may hold values from -0.125 to 0.125
- out_weight: bfloat16 [2048, 2048], P(None, 'tp'), may hold values from -0.125 to 0.125
- chosen: int32 [384, 16], P('kv'), may hold values from 0 to 383, as said below
Outputs:
- mixed: bfloat16 [24576, 2048], P('kv', 'tp')
Inputs may be any that keep to these rules, and one draw needn't show every extreme that they name: `chosen`: row b names no block after b; its first entry is b and its next 3 entries are blocks of the same device as block b; entries may repeat. Over the rows of one device, the entries after the first 4 name at most 2 blocks, counting repeats, of any one other device, and some device names exactly 2 of another.
All inputs are finite; a program needn't handle non-finite values.
Results may differ from a plain program's by a relative error of at most 0.0072.
Values may be sent and summed in bfloat16 or wider, within the bound.
A program may use at most 128 MiB of HBM per device.

v0:
```python
import jax
import jax.numpy as jnp
from jax import lax
from jax.sharding import Mesh
from jax.sharding import PartitionSpec as P

HD = 128
BLK = 64
TOPB = 16
KV = ("kv_0", "kv_1")


def from_everyone(value, axis):
    copies = jnp.broadcast_to(value, (lax.axis_size(axis), *value.shape))
    return lax.all_to_all(copies, axis, split_axis=0, concat_axis=0, tiled=True)


def in_order(parts, dim):
    lengths = list(parts.shape[1:])
    lengths[dim] *= parts.shape[0]
    return jnp.moveaxis(parts, 0, dim).reshape(lengths)


def gathered_copies(value, axis, dim):
    parts = from_everyone(value, axis)
    return in_order(parts, dim)


def gather_axes(value, axes, dim):
    result = value
    for number in range(len(axes) - 1, -1, -1):
        result = lax.all_gather(result, axes[number], axis=dim, tiled=True)
    return result


def local(tokens, query_weight, key_weight, value_weight, out_weight, chosen):
    tok_rows = tokens.shape[0]
    query_cols = query_weight.shape[1]
    key_cols = key_weight.shape[1]
    key_heads = key_cols // HD
    query_heads = query_cols // HD
    group_size = query_heads // key_heads
    own_blocks = tok_rows // BLK
    device = lax.axis_index(KV)
    section = gathered_copies(tokens, "tp", 1)
    query_sum = jnp.dot(section, query_weight, preferred_element_type=jnp.float32)
    key_sum = jnp.dot(section, key_weight, preferred_element_type=jnp.float32)
    value_sum = jnp.dot(section, value_weight, preferred_element_type=jnp.float32)
    queries = query_sum.astype(jnp.bfloat16)
    paired = jnp.concatenate([key_sum.astype(jnp.bfloat16), value_sum.astype(jnp.bfloat16)], axis=1)
    wanted = chosen.reshape(-1)
    everyone = gather_axes(paired, KV, 0)
    fetched = jnp.take(everyone.reshape(-1, BLK, 2 * key_cols), wanted, axis=0)
    fetched = fetched.reshape(own_blocks, TOPB * BLK, 2 * key_cols)
    got_keys = fetched[:, :, :key_cols].reshape(own_blocks, TOPB * BLK, key_heads, HD)
    got_values = fetched[:, :, key_cols:].reshape(own_blocks, TOPB * BLK, key_heads, HD)
    grouped = queries.reshape(own_blocks, BLK, key_heads, group_size, HD)
    scores = jnp.einsum(
        "bqkgd,bskd->bkgqs", grouped, got_keys, preferred_element_type=jnp.float32
    ) * HD ** (-0.5)
    slot_order = jnp.arange(TOPB)
    repeats = jnp.any(
        (chosen[:, :, None] == chosen[:, None, :])
        & (slot_order[None, None, :] < slot_order[None, :, None]),
        axis=2,
    )
    first_block = device * own_blocks
    query_pos = (first_block + jnp.arange(own_blocks))[:, None] * BLK + jnp.arange(BLK)[None, :]
    key_pos = (chosen[:, :, None] * BLK + jnp.arange(BLK)[None, None, :]).reshape(
        own_blocks, TOPB * BLK
    )
    fresh_slot = jnp.broadcast_to((~repeats)[:, :, None], (own_blocks, TOPB, BLK)).reshape(
        own_blocks, TOPB * BLK
    )
    visible = fresh_slot[:, None, :] & (key_pos[:, None, :] <= query_pos[:, :, None])
    scores = jnp.where(visible[:, None, None], scores, -jnp.inf)
    row_peak = jnp.max(scores, axis=-1, keepdims=True)
    weights = jnp.exp(scores - row_peak)
    row_total = jnp.sum(weights, axis=-1)
    mixed_heads = jnp.einsum(
        "bkgqs,bskd->bqkgd",
        weights.astype(jnp.bfloat16),
        got_values,
        preferred_element_type=jnp.float32,
    )
    mixed_heads = mixed_heads / jnp.transpose(row_total, (0, 3, 1, 2))[..., None]
    heads_out = mixed_heads.astype(jnp.bfloat16).reshape(tok_rows, query_cols)
    result = jnp.dot(
        gathered_copies(heads_out, "tp", 1), out_weight, preferred_element_type=jnp.float32
    )
    return result.astype(jnp.bfloat16)


def solution(mesh):
    finer = Mesh(mesh.devices.reshape(16, 4, mesh.shape["tp"]), ("kv_0", "kv_1", "tp"))
    placed = (P(KV, "tp"), P(None, "tp"), P(None, "tp"), P(None, "tp"), P(None, "tp"), P(KV, None))
    return jax.shard_map(local, mesh=finer, in_specs=placed, out_specs=P(KV, "tp"), check_vma=False)
```

profile of v0, /device:TPU:1, one launch (start us, length us, event | category | flops | bytes accessed | tf_op | source)
XLA Modules:
  0.0 265.5 jit_solution(1811074208859304414)
XLA Ops:
  6.5 0.0 copy-start
  6.5 0.0 copy-start.3
  6.5 0.0 all-gather.2.cloned.1.call-start
  6.5 1.2 copy.14
  7.8 0.1 broadcast_in_dim.53
  7.9 0.0 copy-start.4
  7.9 30.0 %all_to_all.10 = bf16[8,384,256]{1,2,0:T(8,128)(2,1)S(1)} all-to-all(bf16[8,384,256]{1,2,0:T(8,128)(2,1)S(1)} %broadcast_in_dim.53), channel_id=1, replica_groups=mesh['kv_0'=16,'kv_1'=4,'tp'=8] {'tp'}, dimensions={0} | all-to-all | bytes 3145728 | tf_op jit(solution)/shard_map/all_to_all | solution.py:15
  37.9 0.0 copy-done.3
  37.9 0.5 convolution_convert_fusion.2
  38.4 0.0 copy-done.4
  38.4 0.0 copy-start.2
  38.4 0.5 convolution_convert_fusion.3
  38.9 11.5 %all_gather.6 = bf16[1536,256]{0,1:T(8,128)(2,1)} all-gather(bf16[384,256]{0,1:T(8,128)(2,1)S(1)} %pad_maximum_fusion), channel_id=1, replica_groups=mesh['kv_0'=16,'kv_1'=4,'tp'=8] {'kv_1'}, dimensions={0}, use_global_device_ids=true | all-gather | bytes 983040 | tf_op jit(solution)/shard_map/all_gather | solution.py:32
  50.4 0.0 all-gather.2.cloned.1.call-update
  50.4 0.0 copy-done.2
  50.5 0.1 reshape.150
  50.5 0.1 add.79
  50.6 0.1 add.80
  50.7 0.1 add.82
  50.8 0.3 and_reduce_fusion
  51.1 0.1 broadcast_in_dim.55
  51.1 0.1 and.35
  51.3 0.1 broadcast_in_dim.50
  51.3 0.1 broadcast_in_dim.51
  51.5 0.1 iota_add_fusion
  51.6 0.4 compare_and_fusion
  51.9 0.0 copy-done
  51.9 0.6 convolution_convert_fusion.1
  52.6 0.1 reshape.151
  52.6 149.0 %all-gather.2.cloned.1.call-done = bf16[24576,256]{0,1:T(8,128)(2,1)} async-done(((bf16[1536,256]{0,1:T(8,128)(2,1)}), bf16[24576,256]{0,1:T(8,128)(2,1)}) %all-gather.2.cloned.1.call-update) | async-done | bytes 12582928 | tf_op jit(solution)/shard_map/all_gather | solution.py:32
  201.6 16.6 %copy.15 = bf16[24576,256]{1,0:T(8,128)(2,1)} copy(bf16[24576,256]{0,1:T(8,128)(2,1)} %all-gather.2.cloned.1.call-done) | data formatting | bytes 25165824 | tf_op jit(solution)/shard_map/all_gather | solution.py:32
  218.3 7.1 %gather_fusion = bf16[96,64,256]{2,1,0:T(8,128)(2,1)} fusion(bf16[384,64,256]{2,1,0:T(8,128)(2,1)} %bitcast.85, s32[1024]{0:T(1024)S(1)} %pad_clamp_fusion), kind=kCustom, calls=%fused_computation | custom fusion | bytes 6291840 | tf_op jit(solution)/shard_map/jit(_take)/gather | solution.py:53
  225.4 3.2 %bitcast_select_fusion.1 = bf16[6,1024,256]{2,1,0:T(8,128)(2,1)S(1)} fusion(pred[6,1024]{1,0:T(8,128)(4,1)S(1)} %broadcast_in_dim.51, bf16[6,1024,256]{2,1,0:T(8,128)(2,1)} %bitcast.86), kind=kLoop, calls=%fused_computation.2 | loop fusion | flops 1572864 | bytes 6297600 | tf_op jit(solution)/shard_map/jit(_take)/select_n | solution.py:53
  228.6 0.8 fusion.2
  229.4 0.9 fusion
  230.3 1.1 fusion.17
  231.4 0.0 copy-start.1
  231.4 0.2 copy.17
  231.6 0.2 copy.18
  231.8 0.1 broadcast_in_dim.58
  231.9 25.4 %all_to_all.11 = bf16[8,384,256]{1,2,0:T(8,128)(2,1)S(1)} all-to-all(bf16[8,384,256]{1,2,0:T(8,128)(2,1)S(1)} %broadcast_in_dim.58), channel_id=1, replica_groups=mesh['kv_0'=16,'kv_1'=4,'tp'=8] {'tp'}, dimensions={0} | all-to-all | bytes 3145728 | tf_op jit(solution)/shard_map/all_to_all | solution.py:15
  257.4 0.0 copy-done.1
  257.4 1.3 convolution_convert_fusion
  (11 shorter events, 0.1 us)
Async XLA Ops:
  6.5 45.4 %copy-start = (bf16[2048,256]{1,0:T(8,128)(2,1)S(1)}, bf16[2048,256]{1,0:T(8,128)(2,1)}, u32[]{:S(2)}) copy-start(bf16[2048,256]{1,0:T(8,128)(2,1)} %param.7) | copy-start | bytes 3145732
  6.5 31.3 %copy-start.3 = (bf16[2048,128]{1,0:T(8,128)(2,1)S(1)}, bf16[2048,128]{1,0:T(8,128)(2,1)}, u32[]{:S(2)}) copy-start(bf16[2048,128]{1,0:T(8,128)(2,1)} %param.9) | copy-start | bytes 1572868
  6.5 195.1 %all-gather.2.cloned.1.call-start = ((), (), s32[]{:S(2)}) async-start(), calls=%async_computation.2 | async-start | bytes 13369344 | tf_op jit(solution)/shard_map/all_gather | solution.py:32
  7.9 30.5 %copy-start.4 = (bf16[2048,128]{1,0:T(8,128)(2,1)S(1)}, bf16[2048,128]{1,0:T(8,128)(2,1)}, u32[]{:S(2)}) copy-start(bf16[2048,128]{1,0:T(8,128)(2,1)} %param.8) | copy-start | bytes 1572868
  38.4 12.1 %copy-start.2 = (s32[6,16]{1,0:T(8,128)S(1)}, s32[6,16]{1,0:T(8,128)}, u32[]{:S(2)}) copy-start(s32[6,16]{1,0:T(8,128)} %param.11) | copy-start | bytes 1156
  231.4 26.0 %copy-start.1 = (bf16[2048,256]{1,0:T(8,128)(2,1)S(1)}, bf16[2048,256]{1,0:T(8,128)(2,1)}, u32[]{:S(2)}) copy-start(bf16[2048,256]{1,0:T(8,128)(2,1)} %param.10) | copy-start | bytes 3145732
Sparse Core Ops, SparseCore 0:
  50.6 151.0 all-gather.1
where the time goes:
time: 266 us
  waiting for transfers between devices  149 us (56%)
  blocking collectives  66.9 us (25%)
  local copies, waits for them, and re-layouts  26.4 us (10%)
  between operations  13.6 us (5%)
  other arithmetic  4.84 us (2%)
  matrix products  4.74 us (2%)
    all_gather x1, waiting for transfers between devices, gather_axes(): result = lax.all_gather(result, axes[number], axis=dim, tiled=True)  149 us
    all_to_all x2, blocking collectives, from_everyone(): return lax.all_to_all(copies, axis, split_axis=0, concat_axis=0, tiled=True)  55.4 us
    all_gather x1, local copies, waits for them, and re-layouts, gather_axes(): result = lax.all_gather(result, axes[number], axis=dim, tiled=True)  16.6 us
    all_gather x1, blocking collectives, gather_axes(): result = lax.all_gather(result, axes[number], axis=dim, tiled=True)  11.5 us
    gather x1, local copies, waits for them, and re-layouts, local(): fetched = jnp.take(everyone.reshape(-1, BLK, 2 * key_cols), wanted, axis=0)  7.13 us
  transfers between devices with their start and end apart: 1, of which 1 were waited for; matrix products, arithmetic and copies ran while one was open for 1% of the time, Pallas kernels for 0%

commit v1 on v0

v1 whole, which is shorter than its diff:
```python
import math

import jax
import jax.numpy as jnp
from jax import lax
from jax.experimental import pallas as pl
from jax.experimental.pallas import tpu as pltpu
from jax.sharding import PartitionSpec as P

HD = 128
BLK = 64
TOPB = 16
NB = 6
NX, NY, NZ = 4, 4, 16
ROWS = NB * BLK
COLS = 256
PER = 10
OWN = NZ * PER
MESH = pl.DeviceIdType.MESH
BF = jnp.bfloat16
F32 = jnp.float32
EXP_SCALE = HD ** (-0.5) * math.log2(math.e)


class Exchange:
    def __init__(self, buf, rows, x, c, kv, ssem, rsem):
        self.buf, self.rows, self.x, self.c, self.kv = buf, rows, x, c, kv
        self.ssem, self.rsem = ssem, rsem
        self.xp, self.xm, self.xo = (x + 1) % NX, (x + NX - 1) % NX, (x + 2) % NX
        self.pc = 1 - c
        self.sent = []

    def part(self, x, c, chunk, half=None):
        rows = self.rows if half is None else self.rows // 2
        start = chunk * self.rows + (0 if half is None else half * rows)
        return self.buf.at[x * 2 + c, pl.ds(start, rows), :]

    def copy(self, ref, chunk, kind, x, c):
        return pltpu.make_async_remote_copy(
            src_ref=ref, dst_ref=ref, send_sem=self.ssem.at[chunk, kind], recv_sem=self.rsem.at[chunk, kind],
            device_id={"kv": self.kv, "tp": x * 2 + c}, device_id_type=MESH,
        )

    def send(self, ref, chunk, kind, x, c):
        copy = self.copy(ref, chunk, kind, x, c)
        copy.start()
        self.sent.append(copy)

    def got(self, ref, chunk, kind):
        self.copy(ref, chunk, kind, self.x, self.pc).wait_recv()

    def own(self, k):
        ref = self.part(self.x, self.c, k)
        self.send(ref, k, 0, self.xp, self.c)
        self.send(ref, k, 1, self.xm, self.c)
        self.send(ref, k, 2, self.x, self.pc)

    def direct(self, k):
        self.got(self.part(self.xm, self.c, k), k, 0)
        self.send(self.part(self.xm, self.c, k, 0), k, 3, self.xp, self.c)
        self.send(self.part(self.xm, self.c, k), k, 5, self.x, self.pc)
        self.got(self.part(self.xp, self.c, k), k, 1)
        self.send(self.part(self.xp, self.c, k, 1), k, 4, self.xm, self.c)
        self.send(self.part(self.xp, self.c, k), k, 6, self.x, self.pc)

    def relayed(self, k):
        for half in (0, 1):
            ref = self.part(self.xo, self.c, k, half)
            self.got(ref, k, 3 + half)
            self.send(ref, k, 7 + half, self.x, self.pc)

    def finish(self, k):
        self.got(self.part(self.x, self.pc, k), k, 2)
        self.got(self.part(self.xm, self.pc, k), k, 5)
        self.got(self.part(self.xp, self.pc, k), k, 6)
        self.got(self.part(self.xo, self.pc, k, 0), k, 7)
        self.got(self.part(self.xo, self.pc, k, 1), k, 8)

    def drain(self):
        for copy in self.sent:
            copy.wait_send()


def kernel(tok, wq, wk, wv, wo, req_in, idx_ref, bias_ref, out_ref, *scratch):
    (xbuf, hbuf, wqkv, wos, qs, own, mid, pool, stage, kvs, rbuf, req_sm) = scratch[:12]
    units_f, units_b = scratch[12:19], scratch[19:26]
    (lsem, a_s, a_r, e_s, e_r, zs, zr, ms, mr, ys, yr, os_, or_, rs, rr, smem_sem) = scratch[26:]

    kv = lax.axis_index("kv")
    tp = lax.axis_index("tp")
    z, y = kv // NY, kv % NY
    x, c = tp // 2, tp % 2
    yp, ym, yo = (y + 1) % NY, (y + NY - 1) % NY, (y + 2) % NY
    zp, zm = (z + 1) % NZ, (z + NZ - 1) % NZ

    loads = [
        pltpu.make_async_copy(tok, xbuf.at[tp], lsem.at[0]),
        pltpu.make_async_copy(wq, wqkv.at[:, 0:256], lsem.at[1]),
        pltpu.make_async_copy(wk, wqkv.at[:, 256:384], lsem.at[2]),
        pltpu.make_async_copy(wv, wqkv.at[:, 384:512], lsem.at[3]),
        pltpu.make_async_copy(wo, wos, lsem.at[4]),
    ]
    for load in loads:
        load.start()

    def dev(zz, yy, tt):
        return {"kv": zz * NY + yy, "tp": tt}

    near = [
        dev(z, y, x * 2 + 1 - c), dev(z, y, ((x + 1) % NX) * 2 + c), dev(z, y, ((x + 3) % NX) * 2 + c),
        dev(z, yp, tp), dev(z, ym, tp), dev(z, yo, tp), dev(zp, y, tp), dev(zm, y, tp),
    ]
    barrier = pltpu.get_barrier_semaphore()
    for other in near:
        pl.semaphore_signal(barrier, inc=1, device_id=other, device_id_type=MESH)
    pl.semaphore_wait(barrier, len(near))

    sent = []

    def rcopy(src, dst, ssem, rsem, to):
        return pltpu.make_async_remote_copy(
            src_ref=src, dst_ref=dst, send_sem=ssem, recv_sem=rsem, device_id=to, device_id_type=MESH
        )

    def send(*args):
        copy = rcopy(*args)
        copy.start()
        sent.append(copy)

    tokens = Exchange(xbuf, 2 * BLK, x, c, kv, a_s, a_r)
    loads[0].wait()
    tokens.own(0)
    tokens.own(1)
    send(req_in.at[yp], rbuf.at[2], rs.at[2], rr.at[2], dev(z, yp, tp))
    send(req_in.at[yo], rbuf.at[1], rs.at[1], rr.at[1], dev(z, yo, tp))
    send(req_in.at[ym], rbuf.at[0], rs.at[0], rr.at[0], dev(z, ym, tp))
    for load in loads[1:]:
        load.wait()

    def project(k):
        rows = pl.ds(k * 2 * BLK, 2 * BLK)
        total = None
        for t in range(8):
            term = jnp.dot(xbuf[t, rows, :], wqkv[t * COLS:(t + 1) * COLS, :], preferred_element_type=F32)
            total = term if total is None else total + term
        rounded = total.astype(BF)
        for i in range(2):
            b = 2 * k + i
            here = rounded[i * BLK:(i + 1) * BLK]
            own[b] = here[:, 256:512]
            pool[OWN + b] = here[:, 256:512]
            qs[b, 0:BLK, :] = here[:, 0:128]
            qs[b, BLK:2 * BLK, :] = here[:, 128:256]

    def piece(s):
        return pl.ds(2 * s, 2)

    def fwd(k, s):
        src = own if k == 1 else units_f[k - 2]
        return (src.at[piece(s)], units_f[k - 1].at[piece(s)], zs.at[0, k - 1, s], zr.at[0, k - 1, s], dev(zp, y, tp))

    def bwd(k, s):
        src = own if k == 1 else units_b[k - 2]
        return (src.at[piece(s)], units_b[k - 1].at[piece(s)], zs.at[1, k - 1, s], zr.at[1, k - 1, s], dev(zm, y, tp))

    def mid_fwd():
        return (units_f[6].at[pl.ds(0, 3)], mid.at[pl.ds(0, 3)], ms.at[0], mr.at[0], dev(zp, y, tp))

    def mid_bwd():
        return (units_b[6].at[pl.ds(3, 3)], mid.at[pl.ds(3, 3)], ms.at[1], mr.at[1], dev(zm, y, tp))

    def finish_chunk(k):
        tokens.finish(k)
        project(k)
        send(*fwd(1, k))
        send(*bwd(1, k))

    tokens.direct(0)
    tokens.own(2)
    tokens.direct(1)
    tokens.relayed(0)
    finish_chunk(0)
    tokens.direct(2)
    tokens.relayed(1)
    finish_chunk(1)
    tokens.relayed(2)
    finish_chunk(2)

    mine = pltpu.make_async_copy(req_in.at[y], req_sm.at[0], smem_sem.at[0])
    mine.start()
    asked = []
    for i in range(3):
        rcopy(rbuf.at[i], rbuf.at[i], rs.at[i], rr.at[i], dev(z, yp, tp)).wait_recv()
        asked.append(pltpu.make_async_copy(rbuf.at[i], req_sm.at[i + 1], smem_sem.at[i + 1]))
        asked[-1].start()
    mine.wait()
    for copy in asked:
        copy.wait()

    def up(d):
        return (stage.at[d, pl.ds(0, 3)], pool.at[pl.ds(d * PER + 2, 3)], ys.at[d, 0], yr.at[d, 0], dev(z, yp, tp))

    def down(d):
        return (stage.at[d, pl.ds(3, 3)], pool.at[pl.ds(d * PER + 5, 3)], ys.at[d, 1], yr.at[d, 1], dev(z, ym, tp))

    def far_up(d):
        return (pool.at[d * PER + 4], pool.at[d * PER + 8], os_.at[d, 0], or_.at[d, 0], dev(z, yp, tp))

    def far_down(d):
        return (pool.at[d * PER + 7], pool.at[d * PER + 9], os_.at[d, 1], or_.at[d, 1], dev(z, ym, tp))

    def pick(unit, d):
        hz = (z + NZ - d) % NZ

        def block(role, slot):
            return unit[req_sm[role, 0, hz * 2 + slot]]

        stage[d, 0] = block(1, 0)
        stage[d, 1] = block(1, 1)
        stage[d, 2] = block(2, 0)
        stage[d, 3] = block(3, 0)
        stage[d, 4] = block(3, 1)
        stage[d, 5] = block(2, 1)
        pool[d * PER] = block(0, 0)
        pool[d * PER + 1] = block(0, 1)
        send(*up(d))
        send(*down(d))

    def relay(d):
        rcopy(*up(d)).wait_recv()
        send(*far_up(d))
        rcopy(*down(d)).wait_recv()
        send(*far_down(d))

    pick(own, 0)
    waiting = [0]
    for k in range(1, 8):
        for s in range(3):
            rcopy(*fwd(k, s)).wait_recv()
            if k < 7:
                send(*fwd(k + 1, s))
            elif s == 1:
                send(*mid_fwd())
            rcopy(*bwd(k, s)).wait_recv()
            if k < 7:
                send(*bwd(k + 1, s))
            elif s == 2:
                send(*mid_bwd())
        pick(units_f[k - 1], k)
        pick(units_b[k - 1], NZ - k)
        for d in waiting:
            relay(d)
        waiting = [k, NZ - k]
    rcopy(*mid_fwd()).wait_recv()
    rcopy(*mid_bwd()).wait_recv()
    pick(mid, 8)
    for d in waiting:
        relay(d)
    relay(8)
    for d in range(NZ):
        rcopy(*far_up(d)).wait_recv()
        rcopy(*far_down(d)).wait_recv()

    heads = Exchange(hbuf, BLK, x, c, kv, e_s, e_r)
    row = lax.broadcasted_iota(jnp.int32, (2 * BLK, 128), 0) % BLK
    col = lax.broadcasted_iota(jnp.int32, (2 * BLK, 128), 1)
    late = (col < BLK) & (col > row)

    def attend(b):
        here = kvs.at[b % 2]
        for j in range(TOPB):
            here[j * BLK:(j + 1) * BLK, :] = pool[idx_ref[b, j]]
        scores = lax.dot_general(
            qs[b], here[:, 0:HD], (((1,), (1,)), ((), ())), preferred_element_type=F32
        ) + bias_ref[b:b + 1, :]
        scores = jnp.concatenate([jnp.where(late, -jnp.inf, scores[:, 0:128]), scores[:, 128:]], axis=1)
        peak = jnp.max(scores, axis=1, keepdims=True)
        weights = jnp.exp2((scores - peak) * EXP_SCALE)
        total = jnp.sum(weights, axis=1, keepdims=True)
        mixed = jnp.dot(weights.astype(BF), here[:, HD:2 * HD], preferred_element_type=F32) / total
        mixed = mixed.astype(BF)
        rows = pl.ds(b * BLK, BLK)
        hbuf[tp, rows, 0:HD] = mixed[0:BLK]
        hbuf[tp, rows, HD:2 * HD] = mixed[BLK:2 * BLK]

    def output(b):
        rows = pl.ds(b * BLK, BLK)
        total = None
        for t in range(8):
            term = jnp.dot(hbuf[t, rows, :], wos[t * COLS:(t + 1) * COLS, :], preferred_element_type=F32)
            total = term if total is None else total + term
        out_ref[rows, :] = total.astype(BF)

    for t in range(NB + 5):
        if t < NB:
            attend(t)
            heads.own(t)
        if 0 <= t - 2 < NB:
            heads.direct(t - 2)
        if 0 <= t - 4 < NB:
            heads.relayed(t - 4)
        if 0 <= t - 5 < NB:
            heads.finish(t - 5)
            output(t - 5)

    tokens.drain()
    heads.drain()
    for copy in sent:
        copy.wait_send()


def tables(chosen):
    device = lax.axis_index("kv")
    z, y = device // NY, device % NY
    holder = chosen // NB
    inner = chosen - holder * NB
    far_holder = holder[:, 4:].reshape(-1)
    far_inner = inner[:, 4:].reshape(-1)
    asked = far_holder[None, :] == jnp.arange(NZ * NY)[:, None]
    low = jnp.min(jnp.where(asked, far_inner[None, :], NB - 1), axis=1)
    high = jnp.max(jnp.where(asked, far_inner[None, :], 0), axis=1)
    both = jnp.stack([low, high], axis=1).reshape(NZ, NY, 2).transpose(1, 0, 2).reshape(NY, 1, 2 * NZ)
    req = jnp.broadcast_to(jnp.pad(both, ((0, 0), (0, 0), (0, 128 - 2 * NZ))), (NY, 8, 128))
    second = jnp.any(
        (far_holder[None, :] == far_holder[:, None]) & (far_inner[None, :] < far_inner[:, None]), axis=1
    ).astype(jnp.int32)
    second = jnp.pad(second.reshape(NB, TOPB - 4), ((0, 0), (4, 0)))
    step = (z - holder // NY) % NZ
    turn = (holder % NY - y) % NY
    place = jnp.where(turn == 0, 0, jnp.where(turn == 1, 5, jnp.where(turn == 2, 8, 2)))
    idx = jnp.where(holder == device, OWN + inner, step * PER + place + second)
    order = jnp.arange(TOPB)
    repeats = jnp.any(
        (chosen[:, :, None] == chosen[:, None, :]) & (order[None, None, :] < order[None, :, None]), axis=2
    )
    bias = jnp.where(repeats, -jnp.inf, 0.0).astype(F32)
    bias = jnp.broadcast_to(bias[:, :, None], (NB, TOPB, BLK)).reshape(NB, TOPB * BLK)
    return req.astype(jnp.int32), idx.astype(jnp.int32), bias


def local(tokens, query_weight, key_weight, value_weight, out_weight, chosen):
    req, idx, bias = tables(chosen)
    dma = pltpu.SemaphoreType.DMA
    hbm = pl.BlockSpec(memory_space=pl.ANY)
    vmem = pl.BlockSpec(memory_space=pltpu.VMEM)
    smem = pl.BlockSpec(memory_space=pltpu.SMEM)
    unit = pltpu.VMEM((NB, BLK, COLS), BF)
    scratch = [
        pltpu.VMEM((8, ROWS, COLS), BF),
        pltpu.VMEM((8, ROWS, COLS), BF),
        pltpu.VMEM((2048, 512), BF),
        pltpu.VMEM((2048, COLS), BF),
        pltpu.VMEM((NB, 2 * BLK, HD), BF),
        unit,
        unit,
        pltpu.VMEM((OWN + NB, BLK, COLS), BF),
        pltpu.VMEM((NZ, 6, BLK, COLS), BF),
        pltpu.VMEM((2, TOPB * BLK, COLS), BF),
        pltpu.VMEM((3, 8, 128), jnp.int32),
        pltpu.SMEM((4, 8, 128), jnp.int32),
        *([unit] * 14),
        dma((5,)),
        dma((3, 9)), dma((3, 9)),
        dma((NB, 9)), dma((NB, 9)),
        dma((2, 7, 3)), dma((2, 7, 3)),
        dma((2,)), dma((2,)),
        dma((NZ, 2)), dma((NZ, 2)),
        dma((NZ, 2)), dma((NZ, 2)),
        dma((3,)), dma((3,)),
        dma((4,)),
    ]
    return pl.pallas_call(
        kernel,
        out_shape=jax.ShapeDtypeStruct((ROWS, COLS), BF),
        in_specs=[hbm, hbm, hbm, hbm, hbm, vmem, smem, vmem],
        out_specs=vmem,
        scratch_shapes=scratch,
        compiler_params=pltpu.CompilerParams(
            collective_id=0, has_side_effects=True, vmem_limit_bytes=48 * 1024 * 1024
        ),
        name="layer",
    )(tokens, query_weight, key_weight, value_weight, out_weight, req, idx, bias)


def solution(mesh):
    placed = (P("kv", "tp"), P(None, "tp"), P(None, "tp"), P(None, "tp"), P(None, "tp"), P("kv", None))
    return jax.shard_map(local, mesh=mesh, in_specs=placed, out_specs=P("kv", "tp"), check_vma=False)
```

time: 266 us -> 105 us (0.39)
  waiting for transfers between devices: 149 us -> 0 us
  Pallas kernels: 0 us -> 96.9 us
  blocking collectives: 66.9 us -> 0 us
  local copies, waits for them, and re-layouts: 26.4 us -> 6.98 us
  between operations: 13.6 us -> 0.05 us
  matrix products: 4.74 us -> 0 us
  other arithmetic: 4.84 us -> 0.67 us
    all_gather x1 -> x0, waiting for transfers between devices: 149 us -> none  [gather_axes(): result = lax.all_gather(result, axes[number], axis=dim, tiled=True)]
    pallas_call x0 -> x1, Pallas kernels: none -> 96.9 us  [local(): pl.pallas_call(kernel, out_shape=jax.ShapeDtypeStruct((ROWS, COLS), BF),...]
    all_to_all x2 -> x0, blocking collectives: 55.4 us -> none  [from_everyone(): return lax.all_to_all(copies, axis, split_axis=0, concat_axis=0, tiled=True)]
    all_gather x1 -> x0, local copies, waits for them, and re-layouts: 16.6 us -> none  [gather_axes(): result = lax.all_gather(result, axes[number], axis=dim, tiled=True)]
    all_gather x1 -> x0, blocking collectives: 11.5 us -> none  [gather_axes(): result = lax.all_gather(result, axes[number], axis=dim, tiled=True)]
    gather x1 -> x0, local copies, waits for them, and re-layouts: 7.13 us -> none  [local(): fetched = jnp.take(everyone.reshape(-1, BLK, 2 * key_cols), wanted, axis=0)]
    dot_general x6 -> x0, matrix products: 4.74 us -> none  [the longest x1 1.3 us: local(): jnp.dot(gathered_copies(heads_out, 'tp', 1), out_weight, preferred_elemen...]
    unnamed x12 -> x13, local copies, waits for them, and re-layouts: 1.26 us -> 5.91 us
  transfers between devices with their start and end apart: 1 -> 0, of which waited for: 1 -> 0; matrix products, arithmetic and copies ran while one was open for 1% -> 0% of each run, Pallas kernels for 0% -> 0%
where the time goes in v1:
time: 105 us
  Pallas kernels  96.9 us (92%)
  local copies, waits for them, and re-layouts  6.98 us (7%)
    pallas_call x1, Pallas kernels, local(): pl.pallas_call(kernel, out_shape=jax.ShapeDtypeStruct((ROWS, COLS), BF),...  96.9 us
    unnamed x13, local copies, waits for them, and re-layouts  5.91 us

profile of v1, /device:TPU:1, one launch (start us, length us, event | category | flops | bytes accessed | tf_op | source)
XLA Modules:
  0.0 104.6 jit_solution(13962399442121377551)
XLA Ops:
  0.0 0.0 copy-start.5
  0.0 0.7 copy-done.5
  0.7 0.3 and_reduce_fusion
  1.0 0.1 slice.6
  1.0 0.1 eq.65
  1.1 0.1 slice.7
  1.2 0.1 broadcast_in_dim.57
  1.3 0.0 copy-start.4
  1.3 0.2 and_reduce_fusion.1
  1.5 0.1 select_reduce_fusion.1
  1.6 0.1 convert_element_type.5
  1.7 0.1 fusion.5.idx_ref
  1.8 0.1 stack.9
  1.8 0.1 copy.15
  1.9 0.1 stack.10
  2.0 0.1 copy.16
  2.1 0.1 copy.17
  2.2 0.1 broadcast_in_dim.67
  2.3 0.1 reshape.40.bias_ref
  2.4 0.1 copy.18
  2.4 0.0 copy-done.4
  2.5 0.0 copy-start
  2.5 1.2 %copy-done = bf16[2048,256]{1,0:T(8,128)(2,1)S(1)} copy-done((bf16[2048,256]{1,0:T(8,128)(2,1)S(1)}, bf16[2048,256]{1,0:T(8,128)(2,1)}, u32[]{:S(2)}) %copy-start) | copy-done | bytes 1048600
  3.7 0.0 copy-start.1
  3.7 1.2 %copy-done.1 = bf16[2048,256]{1,0:T(8,128)(2,1)S(1)} copy-done((bf16[2048,256]{1,0:T(8,128)(2,1)S(1)}, bf16[2048,256]{1,0:T(8,128)(2,1)}, u32[]{:S(2)}) %copy-start.1) | copy-done | bytes 1048600
  4.9 0.0 copy-start.2
  4.9 1.0 copy-done.2
  6.0 0.0 copy-start.3
  6.0 1.0 copy-done.3
  7.0 96.9 %layer.1 = bf16[384,256]{1,0:T(8,128)(2,1)S(1)} custom-call(bf16[384,256]{1,0:T(8,128)(2,1)S(1)} %copy-done.4, bf16[2048,256]{1,0:T(8,128)(2,1)S(1)} %copy-done, bf16[2048,128]{1,0:T(8,128)(2,1)S(1)} %copy-done.2, bf16[2048,128]{1,0:T(8,128)(2,1)S(1)} %copy-done.3, bf16[2048,256]{1,0:T(8,128)(2,1)S(1)} %copy-done.1, ...), custom_call_target="tpu_custom_call" | custom-call | tf_op jit(solution)/shard_map/layer/pallas_call | solution.py:372
  103.9 0.7 copy.20
  (6 shorter events, 0.0 us)
Async XLA Ops:
  0.0 0.7 copy-start.5
  1.3 1.2 %copy-start.4 = (bf16[384,256]{1,0:T(8,128)(2,1)S(1)}, bf16[384,256]{1,0:T(8,128)(2,1)}, u32[]{:S(2)}) copy-start(bf16[384,256]{1,0:T(8,128)(2,1)} %tok.1) | copy-start | bytes 589828
  2.5 1.2 %copy-start = (bf16[2048,256]{1,0:T(8,128)(2,1)S(1)}, bf16[2048,256]{1,0:T(8,128)(2,1)}, u32[]{:S(2)}) copy-start(bf16[2048,256]{1,0:T(8,128)(2,1)} %wq.1) | copy-start | bytes 3145732
  3.7 1.2 %copy-start.1 = (bf16[2048,256]{1,0:T(8,128)(2,1)S(1)}, bf16[2048,256]{1,0:T(8,128)(2,1)}, u32[]{:S(2)}) copy-start(bf16[2048,256]{1,0:T(8,128)(2,1)} %wo.1) | copy-start | bytes 3145732
  4.9 1.0 copy-start.2
  6.0 1.0 copy-start.3

commit v2 on v1

--- a/solution.py
+++ b/solution.py
@@ -122,10 +122,16 @@
             src_ref=src, dst_ref=dst, send_sem=ssem, recv_sem=rsem, device_id=to, device_id_type=MESH
         )
 
-    def send(*args):
+    def send(*args, only=None):
         copy = rcopy(*args)
-        copy.start()
-        sent.append(copy)
+        if only is None:
+            copy.start()
+        else:
+            pl.when(only)(copy.start)
+        sent.append((only, copy))
+
+    def wait(*args, only):
+        pl.when(only)(rcopy(*args).wait_recv)
 
     tokens = Exchange(xbuf, 2 * BLK, x, c, kv, a_s, a_r)
     loads[0].wait()
@@ -152,6 +158,18 @@
             qs[b, 0:BLK, :] = here[:, 0:128]
             qs[b, BLK:2 * BLK, :] = here[:, 128:256]
 
+    def goes_up(k):
+        return (z >= k - 1) & (z < NZ - 1)
+
+    def comes_up(k):
+        return z >= k
+
+    def goes_down(k):
+        return (z + k - 1) % NZ <= 7
+
+    def comes_down(k):
+        return (z + k) % NZ <= 7
+
     def piece(s):
         return pl.ds(2 * s, 2)
 
@@ -172,8 +190,8 @@
     def finish_chunk(k):
         tokens.finish(k)
         project(k)
-        send(*fwd(1, k))
-        send(*bwd(1, k))
+        send(*fwd(1, k), only=goes_up(1))
+        send(*bwd(1, k), only=goes_down(1))
 
     tokens.direct(0)
     tokens.own(2)
@@ -215,51 +233,54 @@
         def block(role, slot):
             return unit[req_sm[role, 0, hz * 2 + slot]]
 
-        stage[d, 0] = block(1, 0)
-        stage[d, 1] = block(1, 1)
-        stage[d, 2] = block(2, 0)
-        stage[d, 3] = block(3, 0)
-        stage[d, 4] = block(3, 1)
-        stage[d, 5] = block(2, 1)
-        pool[d * PER] = block(0, 0)
-        pool[d * PER + 1] = block(0, 1)
-        send(*up(d))
-        send(*down(d))
+        @pl.when(z >= d)
+        def _():
+            stage[d, 0] = block(1, 0)
+            stage[d, 1] = block(1, 1)
+            stage[d, 2] = block(2, 0)
+            stage[d, 3] = block(3, 0)
+            stage[d, 4] = block(3, 1)
+            stage[d, 5] = block(2, 1)
+            pool[d * PER] = block(0, 0)
+            pool[d * PER + 1] = block(0, 1)
+
+        send(*up(d), only=z >= d)
+        send(*down(d), only=z >= d)
 
     def relay(d):
-        rcopy(*up(d)).wait_recv()
-        send(*far_up(d))
-        rcopy(*down(d)).wait_recv()
-        send(*far_down(d))
+        wait(*up(d), only=z >= d)
+        send(*far_up(d), only=z >= d)
+        wait(*down(d), only=z >= d)
+        send(*far_down(d), only=z >= d)
 
     pick(own, 0)
     waiting = [0]
     for k in range(1, 8):
         for s in range(3):
-            rcopy(*fwd(k, s)).wait_recv()
+            wait(*fwd(k, s), only=comes_up(k))
             if k < 7:
-                send(*fwd(k + 1, s))
+                send(*fwd(k + 1, s), only=goes_up(k + 1))
             elif s == 1:
-                send(*mid_fwd())
-            rcopy(*bwd(k, s)).wait_recv()
+                send(*mid_fwd(), only=goes_up(8))
+            wait(*bwd(k, s), only=comes_down(k))
             if k < 7:
-                send(*bwd(k + 1, s))
+                send(*bwd(k + 1, s), only=goes_down(k + 1))
             elif s == 2:
-                send(*mid_bwd())
+                send(*mid_bwd(), only=goes_down(8))
         pick(units_f[k - 1], k)
         pick(units_b[k - 1], NZ - k)
         for d in waiting:
             relay(d)
         waiting = [k, NZ - k]
-    rcopy(*mid_fwd()).wait_recv()
-    rcopy(*mid_bwd()).wait_recv()
+    wait(*mid_fwd(), only=comes_up(8))
+    wait(*mid_bwd(), only=comes_down(8))
     pick(mid, 8)
     for d in waiting:
         relay(d)
     relay(8)
     for d in range(NZ):
-        rcopy(*far_up(d)).wait_recv()
-        rcopy(*far_down(d)).wait_recv()
+        wait(*far_up(d), only=z >= d)
+        wait(*far_down(d), only=z >= d)
 
     heads = Exchange(hbuf, BLK, x, c, kv, e_s, e_r)
     row = lax.broadcasted_iota(jnp.int32, (2 * BLK, 128), 0) % BLK
@@ -291,22 +312,25 @@
             total = term if total is None else total + term
         out_ref[rows, :] = total.astype(BF)
 
-    for t in range(NB + 5):
-        if t < NB:
-            attend(t)
-            heads.own(t)
-        if 0 <= t - 2 < NB:
-            heads.direct(t - 2)
-        if 0 <= t - 4 < NB:
-            heads.relayed(t - 4)
-        if 0 <= t - 5 < NB:
-            heads.finish(t - 5)
-            output(t - 5)
+    for b in range(NB):
+        attend(b)
+        heads.own(b)
+    for b in range(NB):
+        heads.direct(b)
+    for b in range(NB + 1):
+        if b < NB:
+            heads.relayed(b)
+        if b > 0:
+            heads.finish(b - 1)
+            output(b - 1)
 
     tokens.drain()
     heads.drain()
-    for copy in sent:
-        copy.wait_send()
+    for only, copy in sent:
+        if only is None:
+            copy.wait_send()
+        else:
+            pl.when(only)(copy.wait_send)
 
 
 def tables(chosen):
@@ -376,7 +400,7 @@
         out_specs=vmem,
         scratch_shapes=scratch,
         compiler_params=pltpu.CompilerParams(
-            collective_id=0, has_side_effects=True, vmem_limit_bytes=48 * 1024 * 1024
+            collective_id=0, has_side_effects=True, vmem_limit_bytes=62 * 1024 * 1024
         ),
         name="layer",
     )(tokens, query_weight, key_weight, value_weight, out_weight, req, idx, bias)

time: 105 us -> 92 us (0.88)
  the two profiles are of different devices: /device:TPU:1 before, /device:TPU:481 now
where the time goes in v2:
time: 92 us; the launch traced here: 91.8 us
  Pallas kernels  85.9 us (93%)
  local copies, waits for them, and re-layouts  4.6 us (5%)
  other arithmetic  1.26 us (1%)
    pallas_call x1, Pallas kernels, local(): pl.pallas_call(kernel, out_shape=jax.ShapeDtypeStruct((ROWS, COLS), BF),...  85.9 us
    unnamed x3, local copies, waits for them, and re-layouts  2.29 us

profile of v2, /device:TPU:481, one launch (start us, length us, event | category | flops | bytes accessed | tf_op | source)
XLA Modules:
  0.0 91.8 jit_solution(12261088819506349494)
XLA Ops:
  0.0 0.0 copy-start
  0.0 0.7 copy-done
  0.7 0.3 and_reduce_fusion
  1.0 0.1 slice.6
  1.0 0.1 eq.65
  1.1 0.1 slice.7
  1.2 0.1 broadcast_in_dim.57
  1.3 0.2 and_reduce_fusion.1
  1.5 0.1 select_reduce_fusion.1
  1.6 0.1 convert_element_type.5
  1.7 0.7 fusion.5.idx_ref
  2.3 0.1 stack.9
  2.4 0.1 copy.15
  2.5 0.1 stack.10
  2.6 0.1 copy.16
  2.7 0.1 copy.17
  2.8 0.1 broadcast_in_dim.67
  2.9 0.7 reshape.40.bias_ref
  3.6 0.1 copy.18
  3.6 0.6 broadcast_in_dim.62.req_in
  4.3 85.9 %layer.1 = bf16[384,256]{1,0:T(8,128)(2,1)} custom-call(bf16[384,256]{1,0:T(8,128)(2,1)} %tok.1, bf16[2048,256]{1,0:T(8,128)(2,1)} %wq.1, bf16[2048,128]{1,0:T(8,128)(2,1)} %wk.1, bf16[2048,128]{1,0:T(8,128)(2,1)} %wv.1, bf16[2048,256]{1,0:T(8,128)(2,1)} %wo.1, s32[4,8,128]{2,1,0:T(8,128)} %broadcast_in_dim.62.req_in, s32[6,16]{1,0:T(8,128)} %fusion.5.idx_ref, ...), custom_call_target="tpu_custom_call" | custom-call | tf_op jit(solution)/shard_map/layer/pallas_call | solution.py:396
  90.2 1.6 %copy.20 = bf16[384,256]{1,0:T(8,128)(2,1)} copy(bf16[384,256]{1,0:T(8,128)(2,1)} %layer.1) | data formatting | bytes 393216
  (5 shorter events, 0.0 us)
Async XLA Ops:
  0.0 0.7 copy-start

commit v3 on v2

--- a/solution.py
+++ b/solution.py
@@ -14,8 +14,10 @@
 NX, NY, NZ = 4, 4, 16
 ROWS = NB * BLK
 COLS = 256
-PER = 10
+PER = 6
+FAR = 4
 OWN = NZ * PER
+FLOOR = -1e30
 MESH = pl.DeviceIdType.MESH
 BF = jnp.bfloat16
 F32 = jnp.float32
@@ -81,10 +83,12 @@
             copy.wait_send()
 
 
-def kernel(tok, wq, wk, wv, wo, req_in, idx_ref, bias_ref, out_ref, *scratch):
+def kernel(tok, wq, wk, wv, wo, req_in, idx_ref, bias_ref, far_bias, out_ref, *scratch):
     (xbuf, hbuf, wqkv, wos, qs, own, mid, pool, stage, kvs, rbuf, req_sm) = scratch[:12]
     units_f, units_b = scratch[12:19], scratch[19:26]
-    (lsem, a_s, a_r, e_s, e_r, zs, zr, ms, mr, ys, yr, os_, or_, rs, rr, smem_sem) = scratch[26:]
+    (fpool, fkvs, qin, qrel, fbias, ret, lse, back_rel, back, back_lse, acc, mass) = scratch[26:38]
+    (lsem, a_s, a_r, e_s, e_r, zs, zr, ms, mr, ys, yr, rs, rr, smem_sem, q1s, q1r, q2s, q2r, bs, br, b1s, b1r, b2s, b2r,
+     ls, lr) = scratch[38:]
 
     kv = lax.axis_index("kv")
     tp = lax.axis_index("tp")
@@ -140,6 +144,7 @@
     send(req_in.at[yp], rbuf.at[2], rs.at[2], rr.at[2], dev(z, yp, tp))
     send(req_in.at[yo], rbuf.at[1], rs.at[1], rr.at[1], dev(z, yo, tp))
     send(req_in.at[ym], rbuf.at[0], rs.at[0], rr.at[0], dev(z, ym, tp))
+    send(far_bias, fbias, bs.at[0], br.at[0], dev(z, yo, tp))
     for load in loads[1:]:
         load.wait()
 
@@ -204,6 +209,17 @@
     tokens.relayed(2)
     finish_chunk(2)
 
+    def ship(i):
+        to = dev(z, yp, tp) if i == 0 else dev(z, ym, tp)
+        return (qs.at[pl.ds(3 * i, 3)], qrel.at[i], q1s.at[i], q1r.at[i], to)
+
+    def ship_on(i):
+        to = dev(z, yp, tp) if i == 0 else dev(z, ym, tp)
+        return (qrel.at[i], qin.at[pl.ds(3 * i, 3)], q2s.at[i], q2r.at[i], to)
+
+    send(*ship(0))
+    send(*ship(1))
+
     mine = pltpu.make_async_copy(req_in.at[y], req_sm.at[0], smem_sem.at[0])
     mine.start()
     asked = []
@@ -216,16 +232,10 @@
         copy.wait()
 
     def up(d):
-        return (stage.at[d, pl.ds(0, 3)], pool.at[pl.ds(d * PER + 2, 3)], ys.at[d, 0], yr.at[d, 0], dev(z, yp, tp))
+        return (stage.at[d, pl.ds(0, 2)], pool.at[pl.ds(d * PER + 2, 2)], ys.at[d, 0], yr.at[d, 0], dev(z, yp, tp))
 
     def down(d):
-        return (stage.at[d, pl.ds(3, 3)], pool.at[pl.ds(d * PER + 5, 3)], ys.at[d, 1], yr.at[d, 1], dev(z, ym, tp))
-
-    def far_up(d):
-        return (pool.at[d * PER + 4], pool.at[d * PER + 8], os_.at[d, 0], or_.at[d, 0], dev(z, yp, tp))
-
-    def far_down(d):
-        return (pool.at[d * PER + 7], pool.at[d * PER + 9], os_.at[d, 1], or_.at[d, 1], dev(z, ym, tp))
+        return (stage.at[d, pl.ds(2, 2)], pool.at[pl.ds(d * PER + 4, 2)], ys.at[d, 1], yr.at[d, 1], dev(z, ym, tp))
 
     def pick(unit, d):
         hz = (z + NZ - d) % NZ
@@ -237,24 +247,17 @@
         def _():
             stage[d, 0] = block(1, 0)
             stage[d, 1] = block(1, 1)
-            stage[d, 2] = block(2, 0)
-            stage[d, 3] = block(3, 0)
-            stage[d, 4] = block(3, 1)
-            stage[d, 5] = block(2, 1)
+            stage[d, 2] = block(3, 0)
+            stage[d, 3] = block(3, 1)
+            fpool[2 * d] = block(2, 0)
+            fpool[2 * d + 1] = block(2, 1)
             pool[d * PER] = block(0, 0)
             pool[d * PER + 1] = block(0, 1)
 
         send(*up(d), only=z >= d)
         send(*down(d), only=z >= d)
 
-    def relay(d):
-        wait(*up(d), only=z >= d)
-        send(*far_up(d), only=z >= d)
-        wait(*down(d), only=z >= d)
-        send(*far_down(d), only=z >= d)
-
     pick(own, 0)
-    waiting = [0]
     for k in range(1, 8):
         for s in range(3):
             wait(*fwd(k, s), only=comes_up(k))
@@ -269,23 +272,49 @@
                 send(*mid_bwd(), only=goes_down(8))
         pick(units_f[k - 1], k)
         pick(units_b[k - 1], NZ - k)
-        for d in waiting:
-            relay(d)
-        waiting = [k, NZ - k]
+        if k == 2:
+            for i in range(2):
+                rcopy(*ship(i)).wait_recv()
+                send(*ship_on(i))
     wait(*mid_fwd(), only=comes_up(8))
     wait(*mid_bwd(), only=comes_down(8))
     pick(mid, 8)
-    for d in waiting:
-        relay(d)
-    relay(8)
-    for d in range(NZ):
-        wait(*far_up(d), only=z >= d)
-        wait(*far_down(d), only=z >= d)
-
     heads = Exchange(hbuf, BLK, x, c, kv, e_s, e_r)
     row = lax.broadcasted_iota(jnp.int32, (2 * BLK, 128), 0) % BLK
     col = lax.broadcasted_iota(jnp.int32, (2 * BLK, 128), 1)
     late = (col < BLK) & (col > row)
+
+    def back_first(b):
+        to = dev(z, yp, tp) if b % 2 == 0 else dev(z, ym, tp)
+        return (ret.at[b], back_rel.at[b], b1s.at[b], b1r.at[b], to)
+
+    def back_on(b):
+        to = dev(z, yp, tp) if b % 2 == 0 else dev(z, ym, tp)
+        return (back_rel.at[b], back.at[b], b2s.at[b], b2r.at[b], to)
+
+    def back_mass(b):
+        return (lse.at[b], back_lse.at[b], ls.at[b], lr.at[b], dev(z, yo, tp))
+
+    def attend_far(b):
+        here = fkvs.at[b % 2]
+        for j in range(FAR, TOPB):
+            here[(j - FAR) * BLK:(j - FAR + 1) * BLK, :] = fpool[req_sm[2, 1, b * TOPB + j]]
+        scores = lax.dot_general(
+            qin[b], here[:, 0:HD], (((1,), (1,)), ((), ())), preferred_element_type=F32
+        ) + fbias[b:b + 1, FAR * BLK:]
+        peak = jnp.maximum(jnp.max(scores, axis=1, keepdims=True), FLOOR)
+        weights = jnp.exp2((scores - peak) * EXP_SCALE)
+        total = jnp.maximum(jnp.sum(weights, axis=1, keepdims=True), 1e-30)
+        part = jnp.dot(weights.astype(BF), here[:, HD:2 * HD], preferred_element_type=F32) / total
+        ret[b] = part.astype(BF)
+        size = peak * EXP_SCALE + jnp.log(total) * math.log2(math.e)
+        lse[b] = jnp.transpose(jnp.broadcast_to(size, (2 * BLK, 128)))[0:8]
+        send(*back_first(b))
+        send(*back_mass(b))
+
+    def pass_back(b):
+        rcopy(*back_first(b)).wait_recv()
+        send(*back_on(b))
 
     def attend(b):
         here = kvs.at[b % 2]
@@ -297,8 +326,18 @@
         scores = jnp.concatenate([jnp.where(late, -jnp.inf, scores[:, 0:128]), scores[:, 128:]], axis=1)
         peak = jnp.max(scores, axis=1, keepdims=True)
         weights = jnp.exp2((scores - peak) * EXP_SCALE)
-        total = jnp.sum(weights, axis=1, keepdims=True)
-        mixed = jnp.dot(weights.astype(BF), here[:, HD:2 * HD], preferred_element_type=F32) / total
+        acc[b] = jnp.dot(weights.astype(BF), here[:, HD:2 * HD], preferred_element_type=F32)
+        mass[b, 0] = jnp.broadcast_to(peak * EXP_SCALE, (2 * BLK, 128))
+        mass[b, 1] = jnp.broadcast_to(jnp.sum(weights, axis=1, keepdims=True), (2 * BLK, 128))
+
+    def merge(b):
+        rcopy(*back_on(b)).wait_recv()
+        rcopy(*back_mass(b)).wait_recv()
+        size = jnp.transpose(jnp.broadcast_to(back_lse[b, 0:1, :], (128, 2 * BLK)))
+        peak = mass[b, 0]
+        top = jnp.maximum(peak, size)
+        mine, theirs = jnp.exp2(peak - top), jnp.exp2(size - top)
+        mixed = (acc[b] * mine + back[b].astype(F32) * theirs) / (mass[b, 1] * mine + theirs)
         mixed = mixed.astype(BF)
         rows = pl.ds(b * BLK, BLK)
         hbuf[tp, rows, 0:HD] = mixed[0:BLK]
@@ -312,8 +351,23 @@
             total = term if total is None else total + term
         out_ref[rows, :] = total.astype(BF)
 
+    for i in range(2):
+        rcopy(*ship_on(i)).wait_recv()
+    rcopy(far_bias, fbias, bs.at[0], br.at[0], dev(z, yo, tp)).wait_recv()
     for b in range(NB):
+        attend_far(b)
+    for d in range(NZ):
+        wait(*up(d), only=z >= d)
+        wait(*down(d), only=z >= d)
+    attend(0)
+    attend(1)
+    pass_back(0)
+    pass_back(1)
+    for b in range(2, NB):
         attend(b)
+        pass_back(b)
+    for b in range(NB):
+        merge(b)
         heads.own(b)
     for b in range(NB):
         heads.direct(b)
@@ -344,26 +398,35 @@
     low = jnp.min(jnp.where(asked, far_inner[None, :], NB - 1), axis=1)
     high = jnp.max(jnp.where(asked, far_inner[None, :], 0), axis=1)
     both = jnp.stack([low, high], axis=1).reshape(NZ, NY, 2).transpose(1, 0, 2).reshape(NY, 1, 2 * NZ)
-    req = jnp.broadcast_to(jnp.pad(both, ((0, 0), (0, 0), (0, 128 - 2 * NZ))), (NY, 8, 128))
     second = jnp.any(
         (far_holder[None, :] == far_holder[:, None]) & (far_inner[None, :] < far_inner[:, None]), axis=1
     ).astype(jnp.int32)
     second = jnp.pad(second.reshape(NB, TOPB - 4), ((0, 0), (4, 0)))
     step = (z - holder // NY) % NZ
     turn = (holder % NY - y) % NY
-    place = jnp.where(turn == 0, 0, jnp.where(turn == 1, 5, jnp.where(turn == 2, 8, 2)))
-    idx = jnp.where(holder == device, OWN + inner, step * PER + place + second)
+    far = turn == 2
+    place = jnp.where(turn == 0, 0, jnp.where(turn == 1, 4, 2))
+    idx = jnp.where(holder == device, OWN + inner, jnp.where(far, OWN, step * PER + place + second))
+    far_idx = jnp.where(far, 2 * step + second, 0).reshape(1, 1, NB * TOPB)
+    far_row = jnp.broadcast_to(jnp.pad(far_idx, ((0, 0), (0, 0), (0, 128 - NB * TOPB))), (NY, 1, 128))
+    req_row = jnp.pad(both, ((0, 0), (0, 0), (0, 128 - 2 * NZ)))
+    req = jnp.concatenate([req_row, far_row, jnp.zeros((NY, 6, 128), jnp.int32)], axis=1)
     order = jnp.arange(TOPB)
     repeats = jnp.any(
         (chosen[:, :, None] == chosen[:, None, :]) & (order[None, None, :] < order[None, :, None]), axis=2
     )
-    bias = jnp.where(repeats, -jnp.inf, 0.0).astype(F32)
-    bias = jnp.broadcast_to(bias[:, :, None], (NB, TOPB, BLK)).reshape(NB, TOPB * BLK)
-    return req.astype(jnp.int32), idx.astype(jnp.int32), bias
+    near_bias = jnp.where(repeats | far, -jnp.inf, 0.0).astype(F32)
+    far_bias = jnp.where(far & ~repeats, 0.0, -jnp.inf).astype(F32)
+
+    def spread(rows):
+        return jnp.broadcast_to(rows[:, :, None], (NB, TOPB, BLK)).reshape(NB, TOPB * BLK)
+
+    far_bias = jnp.pad(spread(far_bias), ((0, 2), (0, 0)))
+    return req.astype(jnp.int32), idx.astype(jnp.int32), spread(near_bias), far_bias
 
 
 def local(tokens, query_weight, key_weight, value_weight, out_weight, chosen):
-    req, idx, bias = tables(chosen)
+    req, idx, bias, far_bias = tables(chosen)
     dma = pltpu.SemaphoreType.DMA
     hbm = pl.BlockSpec(memory_space=pl.ANY)
     vmem = pl.BlockSpec(memory_space=pltpu.VMEM)
@@ -378,32 +441,47 @@
         unit,
         unit,
         pltpu.VMEM((OWN + NB, BLK, COLS), BF),
-        pltpu.VMEM((NZ, 6, BLK, COLS), BF),
+        pltpu.VMEM((NZ, 4, BLK, COLS), BF),
         pltpu.VMEM((2, TOPB * BLK, COLS), BF),
         pltpu.VMEM((3, 8, 128), jnp.int32),
         pltpu.SMEM((4, 8, 128), jnp.int32),
         *([unit] * 14),
+        pltpu.VMEM((2 * NZ, BLK, COLS), BF),
+        pltpu.VMEM((2, (TOPB - FAR) * BLK, COLS), BF),
+        pltpu.VMEM((NB, 2 * BLK, HD), BF),
+        pltpu.VMEM((2, 3, 2 * BLK, HD), BF),
+        pltpu.VMEM((8, TOPB * BLK), F32),
+        pltpu.VMEM((NB, 2 * BLK, HD), BF),
+        pltpu.VMEM((NB, 8, 128), F32),
+        pltpu.VMEM((NB, 2 * BLK, HD), BF),
+        pltpu.VMEM((NB, 2 * BLK, HD), BF),
+        pltpu.VMEM((NB, 8, 128), F32),
+        pltpu.VMEM((NB, 2 * BLK, HD), F32),
+        pltpu.VMEM((NB, 2, 2 * BLK, 128), F32),
         dma((5,)),
         dma((3, 9)), dma((3, 9)),
         dma((NB, 9)), dma((NB, 9)),
         dma((2, 7, 3)), dma((2, 7, 3)),
         dma((2,)), dma((2,)),
         dma((NZ, 2)), dma((NZ, 2)),
-        dma((NZ, 2)), dma((NZ, 2)),
         dma((3,)), dma((3,)),
         dma((4,)),
+        dma((2,)), dma((2,)), dma((2,)), dma((2,)),
+        dma((1,)), dma((1,)),
+        dma((NB,)), dma((NB,)), dma((NB,)), dma((NB,)),
+        dma((NB,)), dma((NB,)),
     ]
     return pl.pallas_call(
         kernel,
         out_shape=jax.ShapeDtypeStruct((ROWS, COLS), BF),
-        in_specs=[hbm, hbm, hbm, hbm, hbm, vmem, smem, vmem],
+        in_specs=[hbm, hbm, hbm, hbm, hbm, vmem, smem, vmem, vmem],
         out_specs=vmem,
         scratch_shapes=scratch,
         compiler_params=pltpu.CompilerParams(
-            collective_id=0, has_side_effects=True, vmem_limit_bytes=62 * 1024 * 1024
+            collective_id=0, has_side_effects=True, vmem_limit_bytes=53 * 1024 * 1024 + 512 * 1024
         ),
         name="layer",
-    )(tokens, query_weight, key_weight, value_weight, out_weight, req, idx, bias)
+    )(tokens, query_weight, key_weight, value_weight, out_weight, req, idx, bias, far_bias)
 
 
 def solution(mesh):

time: 92 us -> 81.6 us (0.89)
  the two profiles are of different devices: /device:TPU:481 before, /device:TPU:1 now
where the time goes in v3:
time: 81.6 us; the launch traced here: 81.5 us
  Pallas kernels  78 us (96%)
  local copies, waits for them, and re-layouts  2.7 us (3%)
    pallas_call x1, Pallas kernels, local(): pl.pallas_call(kernel, out_shape=jax.ShapeDtypeStruct((ROWS, COLS), BF),...  78 us

profile of v3, /device:TPU:1, one launch (start us, length us, event | category | flops | bytes accessed | tf_op | source)
XLA Modules:
  0.0 81.5 jit_solution(3109415529362353082)
XLA Ops:
  0.0 0.0 copy-start
  0.0 0.1 pad.26.clone
  0.1 0.6 copy-done
  0.7 0.3 and_reduce_fusion
  1.0 0.1 slice.6
  1.1 0.1 eq.64
  1.2 0.1 slice.7
  1.2 0.1 broadcast_in_dim.67
  1.3 0.2 and_reduce_fusion.1
  1.5 0.1 select_reduce_fusion.1
  1.6 0.1 convert_element_type.7
  1.7 0.1 fusion.3
  1.8 0.1 reshape.47
  1.9 0.1 stack.9
  2.0 0.1 copy.15
  2.1 0.1 stack.10
  2.1 0.1 copy.16
  2.2 0.1 copy.17
  2.3 0.1 copy.18
  2.4 0.1 fusion.req_in
  2.5 0.1 broadcast_in_dim.76
  2.6 0.1 reshape.48.bias_ref
  2.7 0.1 broadcast_in_dim.77
  2.7 0.1 reshape.49
  2.8 78.0 %layer.1 = bf16[384,256]{1,0:T(8,128)(2,1)S(1)} custom-call(bf16[384,256]{1,0:T(8,128)(2,1)} %tok.1, bf16[2048,256]{1,0:T(8,128)(2,1)} %wq.1, bf16[2048,128]{1,0:T(8,128)(2,1)} %wk.1, bf16[2048,128]{1,0:T(8,128)(2,1)} %wv.1, bf16[2048,256]{1,0:T(8,128)(2,1)} %wo.1, s32[4,8,128]{2,1,0:T(8,128)S(1)} %fusion.req_in, s32[6,16]{1,0:T(8,128)S(1)} %get-tuple-element.9.idx_ref, ...), custom_call_target="tpu_custom_call" | custom-call | tf_op jit(solution)/shard_map/layer/pallas_call | solution.py:474
  80.8 0.7 copy.20
  (9 shorter events, 0.1 us)
Async XLA Ops:
  0.0 0.7 copy-start

commit v4 on v3

--- a/solution.py
+++ b/solution.py
@@ -86,9 +86,9 @@
 def kernel(tok, wq, wk, wv, wo, req_in, idx_ref, bias_ref, far_bias, out_ref, *scratch):
     (xbuf, hbuf, wqkv, wos, qs, own, mid, pool, stage, kvs, rbuf, req_sm) = scratch[:12]
     units_f, units_b = scratch[12:19], scratch[19:26]
-    (fpool, fkvs, qin, qrel, fbias, ret, lse, back_rel, back, back_lse, acc, mass) = scratch[26:38]
-    (lsem, a_s, a_r, e_s, e_r, zs, zr, ms, mr, ys, yr, rs, rr, smem_sem, q1s, q1r, q2s, q2r, bs, br, b1s, b1r, b2s, b2r,
-     ls, lr) = scratch[38:]
+    (fpool, fkvs, qin, qrel, fbias, ret, lse, far_out, back_lse, acc, mass) = scratch[26:37]
+    (lsem, a_s, a_r, e_s, e_r, zs, zr, ms, mr, ys, yr, rs, rr, smem_sem, q1s, q1r, q2s, q2r, bs, br, b2s, b2r,
+     ls, lr) = scratch[37:]
 
     kv = lax.axis_index("kv")
     tp = lax.axis_index("tp")
@@ -139,8 +139,8 @@
 
     tokens = Exchange(xbuf, 2 * BLK, x, c, kv, a_s, a_r)
     loads[0].wait()
-    tokens.own(0)
-    tokens.own(1)
+    for k in range(3):
+        tokens.own(k)
     send(req_in.at[yp], rbuf.at[2], rs.at[2], rr.at[2], dev(z, yp, tp))
     send(req_in.at[yo], rbuf.at[1], rs.at[1], rr.at[1], dev(z, yo, tp))
     send(req_in.at[ym], rbuf.at[0], rs.at[0], rr.at[0], dev(z, ym, tp))
@@ -198,16 +198,11 @@
         send(*fwd(1, k), only=goes_up(1))
         send(*bwd(1, k), only=goes_down(1))
 
-    tokens.direct(0)
-    tokens.own(2)
-    tokens.direct(1)
-    tokens.relayed(0)
-    finish_chunk(0)
-    tokens.direct(2)
-    tokens.relayed(1)
-    finish_chunk(1)
-    tokens.relayed(2)
-    finish_chunk(2)
+    for k in range(3):
+        tokens.direct(k)
+    for k in range(3):
+        tokens.relayed(k)
+        finish_chunk(k)
 
     def ship(i):
         to = dev(z, yp, tp) if i == 0 else dev(z, ym, tp)
@@ -279,18 +274,13 @@
     wait(*mid_fwd(), only=comes_up(8))
     wait(*mid_bwd(), only=comes_down(8))
     pick(mid, 8)
-    heads = Exchange(hbuf, BLK, x, c, kv, e_s, e_r)
+    heads = Exchange(hbuf, 2 * BLK, x, c, kv, e_s, e_r)
     row = lax.broadcasted_iota(jnp.int32, (2 * BLK, 128), 0) % BLK
     col = lax.broadcasted_iota(jnp.int32, (2 * BLK, 128), 1)
     late = (col < BLK) & (col > row)
 
-    def back_first(b):
-        to = dev(z, yp, tp) if b % 2 == 0 else dev(z, ym, tp)
-        return (ret.at[b], back_rel.at[b], b1s.at[b], b1r.at[b], to)
-
-    def back_on(b):
-        to = dev(z, yp, tp) if b % 2 == 0 else dev(z, ym, tp)
-        return (back_rel.at[b], back.at[b], b2s.at[b], b2r.at[b], to)
+    def back(b):
+        return (ret.at[b], far_out.at[b], b2s.at[b], b2r.at[b], dev(z, yo, tp))
 
     def back_mass(b):
         return (lse.at[b], back_lse.at[b], ls.at[b], lr.at[b], dev(z, yo, tp))
@@ -309,12 +299,8 @@
         ret[b] = part.astype(BF)
         size = peak * EXP_SCALE + jnp.log(total) * math.log2(math.e)
         lse[b] = jnp.transpose(jnp.broadcast_to(size, (2 * BLK, 128)))[0:8]
-        send(*back_first(b))
+        send(*back(b))
         send(*back_mass(b))
-
-    def pass_back(b):
-        rcopy(*back_first(b)).wait_recv()
-        send(*back_on(b))
 
     def attend(b):
         here = kvs.at[b % 2]
@@ -331,20 +317,20 @@
         mass[b, 1] = jnp.broadcast_to(jnp.sum(weights, axis=1, keepdims=True), (2 * BLK, 128))
 
     def merge(b):
-        rcopy(*back_on(b)).wait_recv()
+        rcopy(*back(b)).wait_recv()
         rcopy(*back_mass(b)).wait_recv()
         size = jnp.transpose(jnp.broadcast_to(back_lse[b, 0:1, :], (128, 2 * BLK)))
         peak = mass[b, 0]
         top = jnp.maximum(peak, size)
         mine, theirs = jnp.exp2(peak - top), jnp.exp2(size - top)
-        mixed = (acc[b] * mine + back[b].astype(F32) * theirs) / (mass[b, 1] * mine + theirs)
+        mixed = (acc[b] * mine + far_out[b].astype(F32) * theirs) / (mass[b, 1] * mine + theirs)
         mixed = mixed.astype(BF)
         rows = pl.ds(b * BLK, BLK)
         hbuf[tp, rows, 0:HD] = mixed[0:BLK]
         hbuf[tp, rows, HD:2 * HD] = mixed[BLK:2 * BLK]
 
     def output(b):
-        rows = pl.ds(b * BLK, BLK)
+        rows = pl.ds(b * 2 * BLK, 2 * BLK)
         total = None
         for t in range(8):
             term = jnp.dot(hbuf[t, rows, :], wos[t * COLS:(t + 1) * COLS, :], preferred_element_type=F32)
@@ -359,20 +345,16 @@
     for d in range(NZ):
         wait(*up(d), only=z >= d)
         wait(*down(d), only=z >= d)
-    attend(0)
-    attend(1)
-    pass_back(0)
-    pass_back(1)
-    for b in range(2, NB):
+    for b in range(NB):
         attend(b)
-        pass_back(b)
     for b in range(NB):
         merge(b)
-        heads.own(b)
-    for b in range(NB):
+        if b % 2 == 1:
+            heads.own(b // 2)
+    for b in range(3):
         heads.direct(b)
-    for b in range(NB + 1):
-        if b < NB:
+    for b in range(4):
+        if b < 3:
             heads.relayed(b)
         if b > 0:
             heads.finish(b - 1)
@@ -454,13 +436,12 @@
         pltpu.VMEM((NB, 2 * BLK, HD), BF),
         pltpu.VMEM((NB, 8, 128), F32),
         pltpu.VMEM((NB, 2 * BLK, HD), BF),
-        pltpu.VMEM((NB, 2 * BLK, HD), BF),
         pltpu.VMEM((NB, 8, 128), F32),
         pltpu.VMEM((NB, 2 * BLK, HD), F32),
         pltpu.VMEM((NB, 2, 2 * BLK, 128), F32),
         dma((5,)),
         dma((3, 9)), dma((3, 9)),
-        dma((NB, 9)), dma((NB, 9)),
+        dma((3, 9)), dma((3, 9)),
         dma((2, 7, 3)), dma((2, 7, 3)),
         dma((2,)), dma((2,)),
         dma((NZ, 2)), dma((NZ, 2)),
@@ -468,7 +449,7 @@
         dma((4,)),
         dma((2,)), dma((2,)), dma((2,)), dma((2,)),
         dma((1,)), dma((1,)),
-        dma((NB,)), dma((NB,)), dma((NB,)), dma((NB,)),
+        dma((NB,)), dma((NB,)),
         dma((NB,)), dma((NB,)),
     ]
     return pl.pallas_call(

time: 81.6 us -> 79.1 us (0.969)
  the two profiles are of different devices: /device:TPU:1 before, /device:TPU:353 now
where the time goes in v4:
time: 79.1 us; the launch traced here: 79 us
  Pallas kernels  75.4 us (95%)
  local copies, waits for them, and re-layouts  2.7 us (3%)
    pallas_call x1, Pallas kernels, local(): pl.pallas_call(kernel, out_shape=jax.ShapeDtypeStruct((ROWS, COLS), BF),...  75.4 us

profile of v4, /device:TPU:353, one launch (start us, length us, event | category | flops | bytes accessed | tf_op | source)
XLA Modules:
  0.0 79.0 jit_solution(13109889843440584047)
XLA Ops:
  0.0 0.0 copy-start
  0.0 0.1 pad.26.clone
  0.1 0.6 copy-done
  0.7 0.3 and_reduce_fusion
  1.0 0.1 slice.6
  1.1 0.1 eq.64
  1.2 0.1 slice.7
  1.2 0.1 broadcast_in_dim.67
  1.3 0.2 and_reduce_fusion.1
  1.5 0.1 select_reduce_fusion.1
  1.6 0.1 convert_element_type.7
  1.7 0.1 fusion.3
  1.8 0.1 reshape.47
  1.9 0.1 stack.9
  2.0 0.1 copy.15
  2.1 0.1 stack.10
  2.1 0.1 copy.16
  2.2 0.1 copy.17
  2.3 0.1 copy.18
  2.4 0.1 fusion.req_in
  2.5 0.1 broadcast_in_dim.76
  2.6 0.1 reshape.48.bias_ref
  2.7 0.1 broadcast_in_dim.77
  2.7 0.1 reshape.49
  2.8 75.4 %layer.1 = bf16[384,256]{1,0:T(8,128)(2,1)S(1)} custom-call(bf16[384,256]{1,0:T(8,128)(2,1)} %tok.1, bf16[2048,256]{1,0:T(8,128)(2,1)} %wq.1, bf16[2048,128]{1,0:T(8,128)(2,1)} %wk.1, bf16[2048,128]{1,0:T(8,128)(2,1)} %wv.1, bf16[2048,256]{1,0:T(8,128)(2,1)} %wo.1, s32[4,8,128]{2,1,0:T(8,128)S(1)} %fusion.req_in, s32[6,16]{1,0:T(8,128)S(1)} %get-tuple-element.9.idx_ref, ...), custom_call_target="tpu_custom_call" | custom-call | tf_op jit(solution)/shard_map/layer/pallas_call | solution.py:455
  78.3 0.7 copy.20
  (9 shorter events, 0.1 us)
Async XLA Ops:
  0.0 0.7 copy-start

commit v5 on v4

--- a/solution.py
+++ b/solution.py
@@ -83,12 +83,28 @@
             copy.wait_send()
 
 
-def kernel(tok, wq, wk, wv, wo, req_in, idx_ref, bias_ref, far_bias, out_ref, *scratch):
+def split(name):
+    holder = (name * 10923) >> 16
+    return holder, name - NB * holder
+
+
+def fill_bias(bias, half, b, names, elsewhere):
+    value = []
+    for j, name in enumerate(names):
+        out = elsewhere(split(name)[0])
+        for earlier in names[:j]:
+            out = out | (earlier == name)
+        value.append(jnp.where(out, -jnp.inf, 0.0).astype(F32))
+    for i in range(len(names) // 2):
+        bias[b:b + 1, i * 128:(i + 1) * 128] = jnp.where(half, value[2 * i], value[2 * i + 1])
+
+
+def kernel(tok, wq, wk, wv, wo, chosen_in, out_ref, *scratch):
     (xbuf, hbuf, wqkv, wos, qs, own, mid, pool, stage, kvs, rbuf, req_sm) = scratch[:12]
     units_f, units_b = scratch[12:19], scratch[19:26]
-    (fpool, fkvs, qin, qrel, fbias, ret, lse, far_out, back_lse, acc, mass) = scratch[26:37]
-    (lsem, a_s, a_r, e_s, e_r, zs, zr, ms, mr, ys, yr, rs, rr, smem_sem, q1s, q1r, q2s, q2r, bs, br, b2s, b2r,
-     ls, lr) = scratch[37:]
+    (fpool, fkvs, qin, qrel, fbias, ret, lse, far_out, back_lse, acc, mass, ask, bias, chosen) = scratch[26:40]
+    (lsem, a_s, a_r, e_s, e_r, zs, zr, ms, mr, ys, yr, rs, rr, smem_sem, q1s, q1r, q2s, q2r, b2s, b2r,
+     ls, lr) = scratch[40:]
 
     kv = lax.axis_index("kv")
     tp = lax.axis_index("tp")
@@ -103,8 +119,9 @@
         pltpu.make_async_copy(wk, wqkv.at[:, 256:384], lsem.at[2]),
         pltpu.make_async_copy(wv, wqkv.at[:, 384:512], lsem.at[3]),
         pltpu.make_async_copy(wo, wos, lsem.at[4]),
+        pltpu.make_async_copy(chosen_in, chosen, lsem.at[5]),
     ]
-    for load in loads:
+    for load in (loads[5], *loads[:5]):
         load.start()
 
     def dev(zz, yy, tt):
@@ -117,6 +134,24 @@
     barrier = pltpu.get_barrier_semaphore()
     for other in near:
         pl.semaphore_signal(barrier, inc=1, device_id=other, device_id_type=MESH)
+
+    lane = lax.broadcasted_iota(jnp.int32, (8, 128), 1)
+    sub = lax.broadcasted_iota(jnp.int32, (8, 128), 0)
+    half = lax.broadcasted_iota(jnp.int32, (1, 128), 1) < BLK
+    loads[5].wait()
+    low = jnp.full((8, 128), NB - 1, jnp.int32)
+    high = jnp.zeros((8, 128), jnp.int32)
+    listed = jnp.zeros((8, 128), jnp.int32)
+    for b in range(NB):
+        names = [chosen[b, j] for j in range(TOPB)]
+        for j in range(TOPB):
+            holder, inner = split(names[j])
+            listed = jnp.where(lane == b * TOPB + j, names[j], listed)
+            if j >= FAR:
+                low = jnp.where(lane == holder, jnp.minimum(low, inner), low)
+                high = jnp.where(lane == holder, jnp.maximum(high, inner), high)
+        fill_bias(bias, half, b, names, lambda holder: (holder & (NY - 1)) == yo)
+    ask[...] = jnp.where(sub == 0, low, jnp.where(sub == 1, high, listed))
     pl.semaphore_wait(barrier, len(near))
 
     sent = []
@@ -141,11 +176,10 @@
     loads[0].wait()
     for k in range(3):
         tokens.own(k)
-    send(req_in.at[yp], rbuf.at[2], rs.at[2], rr.at[2], dev(z, yp, tp))
-    send(req_in.at[yo], rbuf.at[1], rs.at[1], rr.at[1], dev(z, yo, tp))
-    send(req_in.at[ym], rbuf.at[0], rs.at[0], rr.at[0], dev(z, ym, tp))
-    send(far_bias, fbias, bs.at[0], br.at[0], dev(z, yo, tp))
-    for load in loads[1:]:
+    send(ask, rbuf.at[2], rs.at[2], rr.at[2], dev(z, yp, tp))
+    send(ask, rbuf.at[1], rs.at[1], rr.at[1], dev(z, yo, tp))
+    send(ask, rbuf.at[0], rs.at[0], rr.at[0], dev(z, ym, tp))
+    for load in loads[1:5]:
         load.wait()
 
     def project(k):
@@ -215,7 +249,7 @@
     send(*ship(0))
     send(*ship(1))
 
-    mine = pltpu.make_async_copy(req_in.at[y], req_sm.at[0], smem_sem.at[0])
+    mine = pltpu.make_async_copy(ask, req_sm.at[0], smem_sem.at[0])
     mine.start()
     asked = []
     for i in range(3):
@@ -236,7 +270,7 @@
         hz = (z + NZ - d) % NZ
 
         def block(role, slot):
-            return unit[req_sm[role, 0, hz * 2 + slot]]
+            return unit[req_sm[role, slot, hz * NY + y]]
 
         @pl.when(z >= d)
         def _():
@@ -271,6 +305,10 @@
             for i in range(2):
                 rcopy(*ship(i)).wait_recv()
                 send(*ship_on(i))
+        if k == 3:
+            for b in range(NB):
+                names = [req_sm[2, 2, b * TOPB + j] for j in range(FAR, TOPB)]
+                fill_bias(fbias, half, b, names, lambda holder: (holder & (NY - 1)) != y)
     wait(*mid_fwd(), only=comes_up(8))
     wait(*mid_bwd(), only=comes_down(8))
     pick(mid, 8)
@@ -285,13 +323,19 @@
     def back_mass(b):
         return (lse.at[b], back_lse.at[b], ls.at[b], lr.at[b], dev(z, yo, tp))
 
+    def step_of(holder):
+        return (z + NZ - (holder >> 2)) & (NZ - 1)
+
     def attend_far(b):
         here = fkvs.at[b % 2]
         for j in range(FAR, TOPB):
-            here[(j - FAR) * BLK:(j - FAR + 1) * BLK, :] = fpool[req_sm[2, 1, b * TOPB + j]]
+            holder, inner = split(req_sm[2, 2, b * TOPB + j])
+            place = 2 * step_of(holder) + (inner != req_sm[2, 0, holder]).astype(jnp.int32)
+            place = jnp.where((holder & (NY - 1)) == y, place, 0)
+            here[(j - FAR) * BLK:(j - FAR + 1) * BLK, :] = fpool[place]
         scores = lax.dot_general(
             qin[b], here[:, 0:HD], (((1,), (1,)), ((), ())), preferred_element_type=F32
-        ) + fbias[b:b + 1, FAR * BLK:]
+        ) + fbias[b:b + 1, :]
         peak = jnp.maximum(jnp.max(scores, axis=1, keepdims=True), FLOOR)
         weights = jnp.exp2((scores - peak) * EXP_SCALE)
         total = jnp.maximum(jnp.sum(weights, axis=1, keepdims=True), 1e-30)
@@ -305,10 +349,19 @@
     def attend(b):
         here = kvs.at[b % 2]
         for j in range(TOPB):
-            here[j * BLK:(j + 1) * BLK, :] = pool[idx_ref[b, j]]
+            holder, inner = split(chosen[b, j])
+            if j < FAR:
+                place = OWN + inner
+            else:
+                turn = holder & (NY - 1)
+                slot = jnp.where(turn == y, 0, jnp.where(turn == yp, 4, 2))
+                slot = slot + (inner != req_sm[0, 0, holder]).astype(jnp.int32)
+                place = jnp.where(turn == yo, OWN, step_of(holder) * PER + slot)
+                place = jnp.where(holder == kv, OWN + inner, place)
+            here[j * BLK:(j + 1) * BLK, :] = pool[place]
         scores = lax.dot_general(
             qs[b], here[:, 0:HD], (((1,), (1,)), ((), ())), preferred_element_type=F32
-        ) + bias_ref[b:b + 1, :]
+        ) + bias[b:b + 1, :]
         scores = jnp.concatenate([jnp.where(late, -jnp.inf, scores[:, 0:128]), scores[:, 128:]], axis=1)
         peak = jnp.max(scores, axis=1, keepdims=True)
         weights = jnp.exp2((scores - peak) * EXP_SCALE)
@@ -339,7 +392,6 @@
 
     for i in range(2):
         rcopy(*ship_on(i)).wait_recv()
-    rcopy(far_bias, fbias, bs.at[0], br.at[0], dev(z, yo, tp)).wait_recv()
     for b in range(NB):
         attend_far(b)
     for d in range(NZ):
@@ -369,50 +421,10 @@
             pl.when(only)(copy.wait_send)
 
 
-def tables(chosen):
-    device = lax.axis_index("kv")
-    z, y = device // NY, device % NY
-    holder = chosen // NB
-    inner = chosen - holder * NB
-    far_holder = holder[:, 4:].reshape(-1)
-    far_inner = inner[:, 4:].reshape(-1)
-    asked = far_holder[None, :] == jnp.arange(NZ * NY)[:, None]
-    low = jnp.min(jnp.where(asked, far_inner[None, :], NB - 1), axis=1)
-    high = jnp.max(jnp.where(asked, far_inner[None, :], 0), axis=1)
-    both = jnp.stack([low, high], axis=1).reshape(NZ, NY, 2).transpose(1, 0, 2).reshape(NY, 1, 2 * NZ)
-    second = jnp.any(
-        (far_holder[None, :] == far_holder[:, None]) & (far_inner[None, :] < far_inner[:, None]), axis=1
-    ).astype(jnp.int32)
-    second = jnp.pad(second.reshape(NB, TOPB - 4), ((0, 0), (4, 0)))
-    step = (z - holder // NY) % NZ
-    turn = (holder % NY - y) % NY
-    far = turn == 2
-    place = jnp.where(turn == 0, 0, jnp.where(turn == 1, 4, 2))
-    idx = jnp.where(holder == device, OWN + inner, jnp.where(far, OWN, step * PER + place + second))
-    far_idx = jnp.where(far, 2 * step + second, 0).reshape(1, 1, NB * TOPB)
-    far_row = jnp.broadcast_to(jnp.pad(far_idx, ((0, 0), (0, 0), (0, 128 - NB * TOPB))), (NY, 1, 128))
-    req_row = jnp.pad(both, ((0, 0), (0, 0), (0, 128 - 2 * NZ)))
-    req = jnp.concatenate([req_row, far_row, jnp.zeros((NY, 6, 128), jnp.int32)], axis=1)
-    order = jnp.arange(TOPB)
-    repeats = jnp.any(
-        (chosen[:, :, None] == chosen[:, None, :]) & (order[None, None, :] < order[None, :, None]), axis=2
-    )
-    near_bias = jnp.where(repeats | far, -jnp.inf, 0.0).astype(F32)
-    far_bias = jnp.where(far & ~repeats, 0.0, -jnp.inf).astype(F32)
-
-    def spread(rows):
-        return jnp.broadcast_to(rows[:, :, None], (NB, TOPB, BLK)).reshape(NB, TOPB * BLK)
-
-    far_bias = jnp.pad(spread(far_bias), ((0, 2), (0, 0)))
-    return req.astype(jnp.int32), idx.astype(jnp.int32), spread(near_bias), far_bias
-
-
 def local(tokens, query_weight, key_weight, value_weight, out_weight, chosen):
-    req, idx, bias, far_bias = tables(chosen)
     dma = pltpu.SemaphoreType.DMA
     hbm = pl.BlockSpec(memory_space=pl.ANY)
     vmem = pl.BlockSpec(memory_space=pltpu.VMEM)
-    smem = pl.BlockSpec(memory_space=pltpu.SMEM)
     unit = pltpu.VMEM((NB, BLK, COLS), BF)
     scratch = [
         pltpu.VMEM((8, ROWS, COLS), BF),
@@ -432,14 +444,17 @@
         pltpu.VMEM((2, (TOPB - FAR) * BLK, COLS), BF),
         pltpu.VMEM((NB, 2 * BLK, HD), BF),
         pltpu.VMEM((2, 3, 2 * BLK, HD), BF),
-        pltpu.VMEM((8, TOPB * BLK), F32),
+        pltpu.VMEM((8, (TOPB - FAR) * BLK), F32),
         pltpu.VMEM((NB, 2 * BLK, HD), BF),
         pltpu.VMEM((NB, 8, 128), F32),
         pltpu.VMEM((NB, 2 * BLK, HD), BF),
         pltpu.VMEM((NB, 8, 128), F32),
         pltpu.VMEM((NB, 2 * BLK, HD), F32),
         pltpu.VMEM((NB, 2, 2 * BLK, 128), F32),
-        dma((5,)),
+        pltpu.VMEM((8, 128), jnp.int32),
+        pltpu.VMEM((8, TOPB * BLK), F32),
+        pltpu.SMEM((NB, TOPB), jnp.int32),
+        dma((6,)),
         dma((3, 9)), dma((3, 9)),
         dma((3, 9)), dma((3, 9)),
         dma((2, 7, 3)), dma((2, 7, 3)),
@@ -448,21 +463,20 @@
         dma((3,)), dma((3,)),
         dma((4,)),
         dma((2,)), dma((2,)), dma((2,)), dma((2,)),
-        dma((1,)), dma((1,)),
         dma((NB,)), dma((NB,)),
         dma((NB,)), dma((NB,)),
     ]
     return pl.pallas_call(
         kernel,
         out_shape=jax.ShapeDtypeStruct((ROWS, COLS), BF),
-        in_specs=[hbm, hbm, hbm, hbm, hbm, vmem, smem, vmem, vmem],
+        in_specs=[hbm, hbm, hbm, hbm, hbm, hbm],
         out_specs=vmem,
         scratch_shapes=scratch,
         compiler_params=pltpu.CompilerParams(
-            collective_id=0, has_side_effects=True, vmem_limit_bytes=53 * 1024 * 1024 + 512 * 1024
+            collective_id=0, has_side_effects=True, vmem_limit_bytes=53 * 1024 * 1024 + 672 * 1024
         ),
         name="layer",
-    )(tokens, query_weight, key_weight, value_weight, out_weight, req, idx, bias, far_bias)
+    )(tokens, query_weight, key_weight, value_weight, out_weight, chosen)
 
 
 def solution(mesh):

time: 79.1 us -> 76.5 us (0.967)
  local copies, waits for them, and re-layouts: 2.7 us -> 1.37 us
where the time goes in v5:
time: 76.5 us; the launch traced here: 76.4 us
  Pallas kernels  75 us (98%)
  local copies, waits for them, and re-layouts  1.37 us (2%)
    pallas_call x1, Pallas kernels, local(): pl.pallas_call(kernel, out_shape=jax.ShapeDtypeStruct((ROWS, COLS), BF),...  75 us

profile of v5, /device:TPU:353, one launch (start us, length us, event | category | flops | bytes accessed | tf_op | source)
XLA Modules:
  0.0 76.4 jit_solution(8527268215419599973)
XLA Ops:
  0.0 0.0 copy-start
  0.0 0.7 copy-done
  0.7 75.0 %layer.1 = bf16[384,256]{1,0:T(8,128)(2,1)S(1)} custom-call(bf16[384,256]{1,0:T(8,128)(2,1)} %tok.1, bf16[2048,256]{1,0:T(8,128)(2,1)} %wq.1, bf16[2048,128]{1,0:T(8,128)(2,1)} %wk.1, bf16[2048,128]{1,0:T(8,128)(2,1)} %wv.1, bf16[2048,256]{1,0:T(8,128)(2,1)} %wo.1, s32[6,16]{1,0:T(8,128)S(1)} %copy-done), custom_call_target="tpu_custom_call" | custom-call | tf_op jit(solution)/shard_map/layer/pallas_call | solution.py:469
  75.7 0.7 copy.8
Async XLA Ops:
  0.0 0.7 copy-start

commit v6 on v5

--- a/solution.py
+++ b/solution.py
@@ -69,14 +69,13 @@
         for half in (0, 1):
             ref = self.part(self.xo, self.c, k, half)
             self.got(ref, k, 3 + half)
-            self.send(ref, k, 7 + half, self.x, self.pc)
+        self.send(self.part(self.xo, self.c, k), k, 7, self.x, self.pc)
 
     def finish(self, k):
         self.got(self.part(self.x, self.pc, k), k, 2)
         self.got(self.part(self.xm, self.pc, k), k, 5)
         self.got(self.part(self.xp, self.pc, k), k, 6)
-        self.got(self.part(self.xo, self.pc, k, 0), k, 7)
-        self.got(self.part(self.xo, self.pc, k, 1), k, 8)
+        self.got(self.part(self.xo, self.pc, k), k, 7)
 
     def drain(self):
         for copy in self.sent:
@@ -318,10 +317,12 @@
     late = (col < BLK) & (col > row)
 
     def back(b):
-        return (ret.at[b], far_out.at[b], b2s.at[b], b2r.at[b], dev(z, yo, tp))
+        pair = pl.ds(2 * b, 2)
+        return (ret.at[pair], far_out.at[pair], b2s.at[b], b2r.at[b], dev(z, yo, tp))
 
     def back_mass(b):
-        return (lse.at[b], back_lse.at[b], ls.at[b], lr.at[b], dev(z, yo, tp))
+        pair = pl.ds(2 * b, 2)
+        return (lse.at[pair], back_lse.at[pair], ls.at[b], lr.at[b], dev(z, yo, tp))
 
     def step_of(holder):
         return (z + NZ - (holder >> 2)) & (NZ - 1)
@@ -343,8 +344,9 @@
         ret[b] = part.astype(BF)
         size = peak * EXP_SCALE + jnp.log(total) * math.log2(math.e)
         lse[b] = jnp.transpose(jnp.broadcast_to(size, (2 * BLK, 128)))[0:8]
-        send(*back(b))
-        send(*back_mass(b))
+        if b % 2 == 1:
+            send(*back(b // 2))
+            send(*back_mass(b // 2))
 
     def attend(b):
         here = kvs.at[b % 2]
@@ -370,8 +372,9 @@
         mass[b, 1] = jnp.broadcast_to(jnp.sum(weights, axis=1, keepdims=True), (2 * BLK, 128))
 
     def merge(b):
-        rcopy(*back(b)).wait_recv()
-        rcopy(*back_mass(b)).wait_recv()
+        if b % 2 == 0:
+            rcopy(*back(b // 2)).wait_recv()
+            rcopy(*back_mass(b // 2)).wait_recv()
         size = jnp.transpose(jnp.broadcast_to(back_lse[b, 0:1, :], (128, 2 * BLK)))
         peak = mass[b, 0]
         top = jnp.maximum(peak, size)
@@ -455,16 +458,16 @@
         pltpu.VMEM((8, TOPB * BLK), F32),
         pltpu.SMEM((NB, TOPB), jnp.int32),
         dma((6,)),
-        dma((3, 9)), dma((3, 9)),
-        dma((3, 9)), dma((3, 9)),
+        dma((3, 8)), dma((3, 8)),
+        dma((3, 8)), dma((3, 8)),
         dma((2, 7, 3)), dma((2, 7, 3)),
         dma((2,)), dma((2,)),
         dma((NZ, 2)), dma((NZ, 2)),
         dma((3,)), dma((3,)),
         dma((4,)),
         dma((2,)), dma((2,)), dma((2,)), dma((2,)),
-        dma((NB,)), dma((NB,)),
-        dma((NB,)), dma((NB,)),
+        dma((3,)), dma((3,)),
+        dma((3,)), dma((3,)),
     ]
     return pl.pallas_call(
         kernel,

time: 76.5 us -> 75.2 us (0.983)
  the two profiles are of different devices: /device:TPU:353 before, /device:TPU:1 now
where the time goes in v6:
time: 75.2 us; the launch traced here: 74.5 us
  Pallas kernels  73.1 us (97%)
  local copies, waits for them, and re-layouts  1.37 us (2%)
    pallas_call x1, Pallas kernels, local(): pl.pallas_call(kernel, out_shape=jax.ShapeDtypeStruct((ROWS, COLS), BF),...  73.1 us

profile of v6, /device:TPU:1, one launch (start us, length us, event | category | flops | bytes accessed | tf_op | source)
XLA Modules:
  0.0 74.5 jit_solution(8397707445807902635)
XLA Ops:
  0.0 0.0 copy-start
  0.0 0.7 copy-done
  0.7 73.1 %layer.1 = bf16[384,256]{1,0:T(8,128)(2,1)S(1)} custom-call(bf16[384,256]{1,0:T(8,128)(2,1)} %tok.1, bf16[2048,256]{1,0:T(8,128)(2,1)} %wq.1, bf16[2048,128]{1,0:T(8,128)(2,1)} %wk.1, bf16[2048,128]{1,0:T(8,128)(2,1)} %wv.1, bf16[2048,256]{1,0:T(8,128)(2,1)} %wo.1, s32[6,16]{1,0:T(8,128)S(1)} %copy-done), custom_call_target="tpu_custom_call" | custom-call | tf_op jit(solution)/shard_map/layer/pallas_call | solution.py:472
  73.8 0.7 copy.8
Async XLA Ops:
  0.0 0.7 copy-start

commit v7 on v6

--- a/solution.py
+++ b/solution.py
@@ -202,11 +202,11 @@
     def comes_up(k):
         return z >= k
 
-    def goes_down(k):
-        return (z + k - 1) % NZ <= 7
-
-    def comes_down(k):
-        return (z + k) % NZ <= 7
+    def goes_down(k, s):
+        return (z + k - 1) % NZ <= (6 if s == 0 else 7)
+
+    def comes_down(k, s):
+        return (z + k) % NZ <= (6 if s == 0 else 7)
 
     def piece(s):
         return pl.ds(2 * s, 2)
@@ -229,7 +229,7 @@
         tokens.finish(k)
         project(k)
         send(*fwd(1, k), only=goes_up(1))
-        send(*bwd(1, k), only=goes_down(1))
+        send(*bwd(1, k), only=goes_down(1, k))
 
     for k in range(3):
         tokens.direct(k)
@@ -293,11 +293,11 @@
                 send(*fwd(k + 1, s), only=goes_up(k + 1))
             elif s == 1:
                 send(*mid_fwd(), only=goes_up(8))
-            wait(*bwd(k, s), only=comes_down(k))
+            wait(*bwd(k, s), only=comes_down(k, s))
             if k < 7:
-                send(*bwd(k + 1, s), only=goes_down(k + 1))
+                send(*bwd(k + 1, s), only=goes_down(k + 1, s))
             elif s == 2:
-                send(*mid_bwd(), only=goes_down(8))
+                send(*mid_bwd(), only=goes_down(8, 2))
         pick(units_f[k - 1], k)
         pick(units_b[k - 1], NZ - k)
         if k == 2:
@@ -309,7 +309,7 @@
                 names = [req_sm[2, 2, b * TOPB + j] for j in range(FAR, TOPB)]
                 fill_bias(fbias, half, b, names, lambda holder: (holder & (NY - 1)) != y)
     wait(*mid_fwd(), only=comes_up(8))
-    wait(*mid_bwd(), only=comes_down(8))
+    wait(*mid_bwd(), only=comes_down(8, 2))
     pick(mid, 8)
     heads = Exchange(hbuf, 2 * BLK, x, c, kv, e_s, e_r)
     row = lax.broadcasted_iota(jnp.int32, (2 * BLK, 128), 0) % BLK

time: 75.2 us -> 75.2 us (level)
  the two profiles are of different devices: /device:TPU:1 before, /device:TPU:321 now
where the time goes in v7:
time: 75.2 us; the launch traced here: 75 us
  Pallas kernels  73.7 us (98%)
  local copies, waits for them, and re-layouts  1.37 us (2%)
    pallas_call x1, Pallas kernels, local(): pl.pallas_call(kernel, out_shape=jax.ShapeDtypeStruct((ROWS, COLS), BF),...  73.7 us

profile of v7, /device:TPU:321, one launch (start us, length us, event | category | flops | bytes accessed | tf_op | source)
XLA Modules:
  0.0 75.0 jit_solution(14564726967513160587)
XLA Ops:
  0.0 0.0 copy-start
  0.0 0.7 copy-done
  0.7 73.7 %layer.1 = bf16[384,256]{1,0:T(8,128)(2,1)S(1)} custom-call(bf16[384,256]{1,0:T(8,128)(2,1)} %tok.1, bf16[2048,256]{1,0:T(8,128)(2,1)} %wq.1, bf16[2048,128]{1,0:T(8,128)(2,1)} %wk.1, bf16[2048,128]{1,0:T(8,128)(2,1)} %wv.1, bf16[2048,256]{1,0:T(8,128)(2,1)} %wo.1, s32[6,16]{1,0:T(8,128)S(1)} %copy-done), custom_call_target="tpu_custom_call" | custom-call | tf_op jit(solution)/shard_map/layer/pallas_call | solution.py:472
  74.4 0.7 copy.8
Async XLA Ops:
  0.0 0.7 copy-start
